TPU v7x, 512 devices: a whole 4x4x16 slice. The times are simulated.
512 devices in a mesh: sp: 32 (over z, core), tp: 16 (over y, x).
Axes of the slice: x: 4, y: 4, z: 16, core: 2. Of those that a mesh axis runs over, the one named last changes fastest.
Arguments:
- residual_input: bfloat16 [4096, 2048], P(('sp', 'tp')), may hold values from -6 to 6
- mixer_value_input: bfloat16 [4096, 2048], P('sp', 'tp'), may hold values from -6 to 6
- gate_preactivation: bfloat16 [4096, 2048], P('sp', 'tp'), may hold values from -6 to 6
- state_projection_input: bfloat16 [4096, 2, 4, 128], P('sp'), may hold values from -6 to 6
- step_preactivation: bfloat16 [4096, 2, 32], P('sp', None, 'tp'), may hold values from -6 to 6
- spike_log_decay: float32 [4096, 2, 32], P('sp', None, 'tp'), may hold values from -1 to 0
- value_filter_taps: float32 [5, 2048], P(None, 'tp'), may hold values from -2.5 to 2.5
- state_projection_taps: float32 [5, 2, 4, 128], replicated, may hold values from -2.5 to 2.5
- step_size_bias: float32 [2, 32], P(None, 'tp'), may hold values from -0.5 to 0.5
- head_log_decay: float32 [2, 32], P(None, 'tp'), may hold values from -12 to -3
- gated_norm_gain: float32 [2048], P('tp'), may hold values from 0.1 to 1.9
- mixer_output_weight: bfloat16 [2048, 2048], P('tp'), may hold values from -0.125 to 0.125
- feedforward_norm_gain: float32 [2048], replicated, may hold values from 0.1 to 1.9
- routed_expert_index: int32 [4096, 4], P('sp'), may hold values from 0 to 31, all different within a row; in each aligned block of 128 rows (0 to 127, 128 to 255, ...) at most 24 rows name the same one
- routed_expert_weight: float32 [4096, 4], P('sp'), may hold values from 0.2 to 1.2
- routed_gate_weight: bfloat16 [32, 2048, 2048], P('sp', None, 'tp'), may hold values from -0.125 to 0.125
- routed_up_weight: bfloat16 [32, 2048, 2048], P('sp', None, 'tp'), may hold values from -0.125 to 0.125
- routed_down_weight: bfloat16 [32, 2048, 2048], P('sp', 'tp'), may hold values from -0.1875 to 0.1875
- common_gate_weight: bfloat16 [2048, 2048], P(None, 'tp'), may hold values from -0.125 to 0.125
- common_up_weight: bfloat16 [2048, 2048], P(None, 'tp'), may hold values from -0.125 to 0.125
- common_down_weight: bfloat16 [2048, 2048], P('tp'), may hold values from -0.125 to 0.125
Outputs:
- layer_out: bfloat16 [4096, 2048], P(('sp', 'tp'))
Inputs may be any that keep to these rules, and one draw needn't show every extreme that they name: `routed_expert_index`: each row names 4 different experts. In the aligned blocks of 128 rows no expert is named by more than 24 rows, and in some block one expert is named by exactly 24.
All inputs are finite; a program needn't handle non-finite values.
Results may differ from a plain program's by a relative error of at most 0.02.
Values may be sent and summed in bfloat16 or wider, within the bound.
A program may use at most 64 MiB of HBM per device.

v0:
```python
import jax
import jax.numpy as jnp
from jax import lax
from jax.sharding import Mesh
from jax.sharding import PartitionSpec as P

HD = 64
BLK = 128
SP = ("sp_0", "sp_1")
SP_TP = ("sp_0", "sp_1", "tp")


EPSILON = 1e-06
HIGHEST = lax.Precision.HIGHEST


def padded_2(cells, sides, width):
    for axis, dim in sides:
        count = lax.axis_size(axis)
        ends = count - 1
        head = lax.slice_in_dim(cells, 0, width, axis=dim)
        tail = lax.slice_in_dim(cells, cells.shape[dim] - width, cells.shape[dim], axis=dim)
        cells = jnp.concatenate(
            [
                lax.ppermute(tail, axis, [(i, (i + 1) % count) for i in range(ends)]),
                cells,
                lax.ppermute(head, axis, [((i + 1) % count, i) for i in range(ends)]),
            ],
            axis=dim,
        )
    return cells


def neutral_like(value, identity):
    return jax.tree.map(
        lambda part, zero: jnp.zeros_like(part) + jnp.asarray(zero, part.dtype), value, identity
    )


def collected_together(value, axis):
    leaves = jax.tree.leaves(value)
    sequence = sorted(range(len(leaves)), key=lambda k: -leaves[k].size)
    width = (1, *leaves[sequence[0]].shape)[-1]
    lines = [
        jnp.pad(leaves[k].reshape(-1), (0, -leaves[k].size % width)).reshape(-1, width)
        for k in sequence
    ]
    both, at, found = (lax.all_gather(jnp.concatenate(lines), axis), 0, {})
    for k, line in zip(sequence, lines):
        piece = both[:, at : at + len(line)].reshape(len(both), -1)
        found[k] = piece[:, : leaves[k].size].reshape(-1, *leaves[k].shape)
        at += len(line)
    numbers = iter(range(len(leaves)))
    return jax.tree.map(lambda _: found[next(numbers)], value)


def entering(value, axes, combine, identity, reverse):
    before = start = neutral_like(value, identity)
    running = value
    for axis in reversed(axes):
        devices, index = (lax.axis_size(axis), lax.axis_index(axis))
        pieces = collected_together(
            jax.tree.map(
                lambda part, kind: part.astype(kind), running, (jnp.bfloat16, jnp.bfloat16)
            ),
            axis,
        )
        inside, running = (start, start)
        for k in reversed(range(devices)) if reverse else range(devices):
            passed = k > index if reverse else k < index
            running = combine(
                running, jax.tree.map(lambda part, own: part[k].astype(own.dtype), pieces, value)
            )
            inside = jax.tree.map(lambda new, old: jnp.where(passed, new, old), running, inside)
        before = combine(inside, before)
    return before


def cut_along(value, dim, devices):
    dims = value.shape
    pieces = value.reshape(*dims[:dim], devices, dims[dim] // devices, *dims[dim + 1 :])
    return jnp.moveaxis(pieces, dim, 0)


def sum_at_owner(value, axis, dim):
    pieces = cut_along(value, dim, lax.axis_size(axis))
    arrived = lax.all_to_all(pieces, axis, split_axis=0, concat_axis=0, tiled=True)
    return arrived.astype(jnp.float32).sum(axis=0)


def joined_along(pieces, dim):
    pieces = jnp.moveaxis(pieces, 0, dim)
    dims = pieces.shape
    return pieces.reshape(*dims[:dim], dims[dim] * dims[dim + 1], *dims[dim + 2 :])


def sent_to_all(value, axis):
    devices = lax.axis_size(axis)
    return lax.all_to_all(
        jnp.broadcast_to(value[None], (devices, *value.shape)), axis, 0, 0, tiled=True
    )


def gather_directly(value, axis, dim):
    return joined_along(sent_to_all(value, axis), dim)


def rounded(values):
    return lax.optimization_barrier(values.astype(jnp.bfloat16)).astype(jnp.float32)


def block_pass(inputs, decay_logarithm, b_state, c_state, block_len):
    length, groups, per_group, head_dim = inputs.shape
    states = b_state.shape[-1]
    blocks = length // block_len
    inputs = inputs.reshape(blocks, block_len, groups, per_group, head_dim)
    decay_logarithm = decay_logarithm.reshape(blocks, block_len, groups, per_group)
    b_blocks = b_state.reshape(blocks, block_len, groups, states)
    c_blocks = c_state.reshape(blocks, block_len, groups, states)
    within = jnp.cumsum(decay_logarithm, axis=1)
    row_index = lax.broadcasted_iota(jnp.int32, (block_len, block_len), 0)
    col_index = lax.broadcasted_iota(jnp.int32, (block_len, block_len), 1)
    below_mask = (row_index >= col_index)[None, :, :, None, None]
    spread = within[:, :, None] - within[:, None, :]
    weights = jnp.where(below_mask, jnp.exp(jnp.where(below_mask, spread, 0.0)), 0.0)
    scores = jnp.einsum("cign,cjgn->cijg", c_blocks, b_blocks, precision=HIGHEST)
    output = jnp.einsum(
        "cijgr,cjgrp->cigrp", scores[..., None] * weights, inputs, precision=HIGHEST
    )
    tail_decay = jnp.exp(within[:, -1:] - within)
    block_ends = jnp.einsum(
        "cjgn,cjgrp->cgrpn", b_blocks, inputs * tail_decay[..., None], precision=HIGHEST
    )
    totals = within[:, -1]

    def carry_step(carried, pair_item):
        block_total, block_end = pair_item
        return (jnp.exp(block_total)[..., None, None] * carried + block_end, carried)

    zero_state = jnp.zeros((groups, per_group, head_dim, states), jnp.float32)
    last_state, starts = lax.scan(carry_step, zero_state, (totals, block_ends))
    output = (
        output
        + jnp.einsum("cign,cgrpn->cigrp", c_blocks, starts, precision=HIGHEST)
        * jnp.exp(within)[..., None]
    )
    offsets = jnp.cumsum(totals, axis=0) - totals
    through = (within + offsets[:, None]).reshape(length, groups, per_group)
    return (
        output.reshape(length, groups, per_group, head_dim),
        jnp.sum(totals, axis=0),
        last_state,
        through,
    )


def slot_table(expert_ids, experts, capacity):
    row_count, top_count = expert_ids.shape
    flat_ids = expert_ids.reshape(-1)
    one_hot = (flat_ids[:, None] == jnp.arange(experts, dtype=jnp.int32)[None, :]).astype(jnp.int32)
    earlier = jnp.cumsum(one_hot, axis=0) - one_hot
    position = jnp.sum(earlier * one_hot, axis=1)
    owners = jnp.arange(row_count * top_count, dtype=jnp.int32) // top_count
    table = (
        jnp.full((experts * capacity,), row_count, jnp.int32)
        .at[flat_ids * capacity + position]
        .set(owners)
    )
    return (position.reshape(row_count, top_count), table)


def combine_states(earlier, later):
    return (earlier[0] + later[0], jnp.exp(later[0])[..., None, None] * earlier[1] + later[1])


def on_device(
    residual_input,
    mixer_value_input,
    gate_preactivation,
    state_projection_input,
    step_preactivation,
    spike_log_decay,
    value_filter_taps,
    state_projection_taps,
    step_size_bias,
    head_log_decay,
    gated_norm_gain,
    mixer_output_weight,
    feedforward_norm_gain,
    routed_expert_index,
    routed_expert_weight,
    routed_gate_weight,
    routed_up_weight,
    routed_down_weight,
    common_gate_weight,
    common_up_weight,
    common_down_weight,
):
    seq_rows, mixer_cols = mixer_value_input.shape
    heads_dev = mixer_cols // HD
    groups, states = (state_projection_input.shape[2], state_projection_input.shape[3])
    per_group = heads_dev * lax.axis_size("tp") // groups
    group_count = max(1, heads_dev // per_group)
    heads_local = heads_dev // group_count
    first_group = lax.axis_index("tp") * heads_dev // per_group
    taps = value_filter_taps.shape[0]
    margin = taps // 2
    local_bc = lax.dynamic_slice_in_dim(state_projection_input, first_group, group_count, 2)
    local_taps = lax.dynamic_slice_in_dim(state_projection_taps, first_group, group_count, 2)
    joined = jnp.concatenate(
        [mixer_value_input, local_bc.reshape(seq_rows, 2 * group_count * states)], axis=1
    )
    kernel = jnp.concatenate(
        [value_filter_taps, local_taps.reshape(taps, 2 * group_count * states)], axis=1
    )
    padded = padded_2(joined, ((SP, 0),), margin)
    conv_out = jnp.zeros(joined.shape, jnp.float32)
    for offset in range(taps):
        conv_out = conv_out + kernel[offset] * padded[offset : offset + seq_rows].astype(
            jnp.float32
        )
    active = jax.nn.silu(conv_out)
    mixer_values = active[:, :mixer_cols].reshape(seq_rows, group_count, heads_local, HD)
    state_parts = active[:, mixer_cols:].reshape(seq_rows, 2, group_count, states)
    b_state, c_state = (state_parts[:, 0], state_parts[:, 1])
    discrete_step_size = jax.nn.softplus(step_preactivation.astype(jnp.float32) + step_size_bias)
    decay_logarithm = spike_log_decay - discrete_step_size * jnp.exp(head_log_decay)
    forward_in = (
        mixer_values
        * discrete_step_size[:, 0].reshape(seq_rows, group_count, heads_local)[..., None]
    )
    backward_in = (
        mixer_values
        * discrete_step_size[:, 1].reshape(seq_rows, group_count, heads_local)[..., None]
    )
    forward_out, forward_total, forward_end, forward_through = block_pass(
        forward_in,
        decay_logarithm[:, 0].reshape(seq_rows, group_count, heads_local),
        b_state,
        c_state,
        BLK,
    )
    backward_out, backward_total, backward_end, backward_through = block_pass(
        jnp.flip(backward_in, 0),
        jnp.flip(decay_logarithm[:, 1].reshape(seq_rows, group_count, heads_local), 0),
        jnp.flip(b_state, 0),
        jnp.flip(c_state, 0),
        BLK,
    )
    forward_start = entering(
        (forward_total, forward_end),
        SP,
        combine_states,
        (jnp.zeros_like(forward_total), jnp.zeros_like(forward_end)),
        False,
    )[1]
    backward_start = entering(
        (backward_total, backward_end),
        SP,
        combine_states,
        (jnp.zeros_like(backward_total), jnp.zeros_like(backward_end)),
        True,
    )[1]
    forward_out = forward_out + jnp.exp(forward_through)[..., None] * jnp.einsum(
        "lgn,grpn->lgrp", c_state, forward_start, precision=HIGHEST
    )
    backward_out = backward_out + jnp.exp(backward_through)[..., None] * jnp.einsum(
        "lgn,grpn->lgrp", jnp.flip(c_state, 0), backward_start, precision=HIGHEST
    )
    scanned = (forward_out + jnp.flip(backward_out, 0)).reshape(seq_rows, mixer_cols)
    gated = (scanned * jax.nn.silu(gate_preactivation.astype(jnp.float32))).reshape(
        seq_rows, heads_dev, HD
    )
    gated = gated * lax.rsqrt(jnp.mean(gated * gated, axis=-1, keepdims=True) + EPSILON)
    mixed = (gated.reshape(seq_rows, mixer_cols) * gated_norm_gain).astype(jnp.bfloat16)
    picked_rows = mixed
    projected = sum_at_owner(
        rounded(
            jnp.dot(picked_rows, mixer_output_weight, preferred_element_type=jnp.float32)
        ).astype(jnp.bfloat16),
        "tp",
        0,
    )
    residual = (residual_input.astype(jnp.float32) + projected).astype(jnp.bfloat16)
    widened = residual.astype(jnp.float32)
    normed = (
        widened
        * lax.rsqrt(jnp.mean(widened * widened, axis=-1, keepdims=True) + EPSILON)
        * feedforward_norm_gain
    ).astype(jnp.bfloat16)
    all_rows = gather_directly(normed, "tp", 0)
    sp_count = lax.axis_size(SP)
    local_experts = routed_gate_weight.shape[0]
    experts = local_experts * sp_count
    top_count = routed_expert_index.shape[1]
    capacity = 3 * seq_rows * top_count // (2 * experts)
    model_width = all_rows.shape[1]
    position, table = slot_table(routed_expert_index, experts, capacity)
    padded_rows = jnp.concatenate([all_rows, jnp.zeros((1, model_width), jnp.bfloat16)], axis=0)
    column_width = model_width // lax.axis_size("tp")
    own_columns = lax.dynamic_slice_in_dim(
        padded_rows, lax.axis_index("tp") * column_width, column_width, 1
    )
    outgoing = own_columns[table].reshape(sp_count, local_experts, capacity, column_width)
    piece = gather_directly(
        lax.all_to_all(outgoing, SP, split_axis=0, concat_axis=0, tiled=True), "tp", 3
    )
    gate_part = jnp.einsum(
        "secd,edf->secf", piece, routed_gate_weight, preferred_element_type=jnp.float32
    )
    up_part = jnp.einsum(
        "secd,edf->secf", piece, routed_up_weight, preferred_element_type=jnp.float32
    )
    hidden = (jax.nn.silu(gate_part) * up_part).astype(jnp.bfloat16)
    partial_value = lax.optimization_barrier(
        jnp.einsum(
            "secf,efd->secd", hidden, routed_down_weight, preferred_element_type=jnp.float32
        ).astype(jnp.bfloat16)
    ).astype(jnp.float32)
    summed = sum_at_owner(partial_value.astype(jnp.bfloat16), "tp", 3)
    returned = lax.all_to_all(
        summed.astype(jnp.bfloat16), SP, split_axis=0, concat_axis=0, tiled=True
    ).astype(summed.dtype)
    slot_index = routed_expert_index * capacity + position
    flat_back = returned.reshape(experts * capacity, returned.shape[3])
    chosen = flat_back[slot_index]
    routed = jnp.sum(routed_expert_weight[..., None] * chosen, axis=1)
    routed_part = lax.all_to_all(
        routed.astype(jnp.bfloat16), "tp", split_axis=0, concat_axis=1, tiled=True
    ).astype(routed.dtype)
    picked_rows = all_rows
    gate_part = jnp.dot(picked_rows, common_gate_weight, preferred_element_type=jnp.float32)
    up_part = jnp.dot(picked_rows, common_up_weight, preferred_element_type=jnp.float32)
    hidden = (jax.nn.silu(gate_part) * up_part).astype(jnp.bfloat16)
    shared_part = sum_at_owner(
        rounded(jnp.dot(hidden, common_down_weight, preferred_element_type=jnp.float32)).astype(
            jnp.bfloat16
        ),
        "tp",
        0,
    )
    feed = shared_part + routed_part
    return (widened + feed).astype(jnp.bfloat16)


def solution(mesh):
    finer = Mesh(mesh.devices.reshape(16, 2, mesh.shape["tp"]), ("sp_0", "sp_1", "tp"))
    placed = (
        P(SP_TP, None),
        P(SP, "tp"),
        P(SP, "tp"),
        P(SP, None, None, None),
        P(SP, None, "tp"),
        P(SP, None, "tp"),
        P(None, "tp"),
        P(),
        P(None, "tp"),
        P(None, "tp"),
        P("tp"),
        P("tp", None),
        P(),
        P(SP, None),
        P(SP, None),
        P(SP, None, "tp"),
        P(SP, None, "tp"),
        P(SP, "tp", None),
        P(None, "tp"),
        P(None, "tp"),
        P("tp", None),
    )
    return jax.shard_map(
        on_device, mesh=finer, in_specs=placed, out_specs=P(SP_TP, None), check_vma=False
    )
```

profile of v0, /device:TPU:1, one launch (start us, length us, event | category | flops | bytes accessed | tf_op | source)
XLA Modules:
  0.0 321.0 jit_solution(11925908608978256040)
XLA Ops:
  0.0 1.1 constant_dynamic-slice_fusion
  1.2 0.1 copy.169
  1.3 0.9 copy.145
  2.3 4.9 %collective-permute-start = (bf16[2,384]{0,1:T(8,128)(2,1)S(1)}, bf16[2,384]{0,1:T(8,128)(2,1)S(1)}, u32[]{:S(2)}, u32[]{:S(2)}) collective-permute-start(bf16[2,384]{0,1:T(8,128)(2,1)S(1)} %get-tuple-element.50), channel_id=1, source_target_pairs={{0,16},{16,32},{32,48},{48,64},{64,80},{80,96},{96,112},{112,128},... | collective-permute-start | bytes 4616 | tf_op jit(solution)/shard_map/ppermute | solution.py:25
  7.2 5.1 %collective-permute-start.1 = (bf16[2,384]{0,1:T(8,128)(2,1)S(1)}, bf16[2,384]{0,1:T(8,128)(2,1)S(1)}, u32[]{:S(2)}, u32[]{:S(2)}) collective-permute-start(bf16[2,384]{0,1:T(8,128)(2,1)S(1)} %get-tuple-element.51), channel_id=1, source_target_pairs={{16,0},{32,16},{48,32},{64,48},{80,64},{96,80},{112,96},{128,112},... | collective-permute-start | bytes 4616 | tf_op jit(solution)/shard_map/ppermute | solution.py:27
  12.3 0.7 exp.300
  13.0 0.8 multiply_subtract_fusion
  13.9 0.1 copy.153
  14.0 0.1 fusion.199
  14.2 0.1 copy.149
  14.4 0.1 fusion.198
  14.7 0.7 constant_dynamic-update-slice_fusion
  15.4 0.8 dynamic-slice_reduce_fusion
  16.4 0.8 copy.160
  17.3 0.1 maximum_maximum_fusion
  17.4 0.4 divide_multiply_fusion
  17.9 0.3 convolution_bitcast_fusion.9
  18.6 0.3 fusion.12
  18.8 0.3 convolution_bitcast_fusion.5
  19.2 0.2 fusion.16
  19.4 1.9 all-gather.6
  21.8 28.3 %all-gather.7 = bf16[16,129,128]{2,1,0:T(8,128)(2,1)S(1)} all-gather(bf16[1,129,128]{2,1,0:T(8,128)(2,1)S(1)} %maximum_bitcast_fusion.3), channel_id=5, replica_groups=mesh['sp_0'=16,'sp_1'=2,'tp'=16] {'sp_0'}, dimensions={0}, use_global_device_ids=true | all-gather | bytes 561408 | tf_op jit(solution)/shard_map/all_gather | solution.py:48
  52.8 0.4 fusion.5
  53.2 0.4 fusion.45
  53.6 0.3 fusion.14
  54.0 0.2 fusion.8
  54.3 0.3 fusion.15
  54.6 8.6 %all-gather.4 = bf16[2,129,128]{2,1,0:T(8,128)(2,1)S(1)} all-gather(bf16[1,129,128]{2,1,0:T(8,128)(2,1)S(1)} %maximum_bitcast_fusion), channel_id=2, replica_groups=mesh['sp_0'=16,'sp_1'=2,'tp'=16] {'sp_1'}, dimensions={0}, use_global_device_ids=true | all-gather | bytes 99072 | tf_op jit(solution)/shard_map/all_gather | solution.py:48
  63.6 23.3 %all-gather.5 = bf16[16,129,128]{2,1,0:T(8,128)(2,1)S(1)} all-gather(bf16[1,129,128]{2,1,0:T(8,128)(2,1)S(1)} %maximum_bitcast_fusion.1), channel_id=3, replica_groups=mesh['sp_0'=16,'sp_1'=2,'tp'=16] {'sp_0'}, dimensions={0}, use_global_device_ids=true | all-gather | bytes 561408 | tf_op jit(solution)/shard_map/all_gather | solution.py:48
  89.6 0.4 fusion.7
  90.0 0.4 fusion.47
  90.4 0.2 fusion.11
  91.1 1.1 convolution_convert_fusion.2
  92.2 6.8 %all-to-all-start = ((bf16[16,8,2048]{2,1,0:T(8,128)(2,1)}), bf16[16,8,2048]{2,1,0:T(8,128)(2,1)S(1)}, u32[]{:S(2)}, u32[]{:S(2)}) async-start(bf16[16,8,2048]{2,1,0:T(8,128)(2,1)} %bitcast.111), calls=%async_computation | async-start | bytes 1048576 | tf_op jit(solution)/shard_map/all_to_all | solution.py:87
  99.0 1.2 reduce-window.6
  100.2 0.2 slice_reduce_fusion
  100.8 7.1 %all-to-all-done = bf16[16,8,2048]{2,1,0:T(8,128)(2,1)S(1)} async-done(((bf16[16,8,2048]{2,1,0:T(8,128)(2,1)}), bf16[16,8,2048]{2,1,0:T(8,128)(2,1)S(1)}, u32[]{:S(2)}, u32[]{:S(2)}) %all-to-all-start) | async-done | bytes 524320 | tf_op jit(solution)/shard_map/all_to_all | solution.py:87
  108.0 0.1 fusion.60
  108.2 0.8 broadcast_in_dim.53
  109.1 3.6 %all-to-all-start.1 = ((bf16[16,8,2048]{2,1,0:T(8,128)(2,1)}), bf16[16,8,2048]{2,1,0:T(8,128)(2,1)S(1)}, u32[]{:S(2)}, u32[]{:S(2)}) async-start(bf16[16,8,2048]{2,1,0:T(8,128)(2,1)} %broadcast_in_dim.53), calls=%async_computation.1 | async-start | bytes 1048576 | tf_op jit(solution)/shard_map/all_to_all | solution.py:99
  112.7 2.4 scatter_custom_fusion
  115.2 6.4 %all-to-all-done.1 = bf16[16,8,2048]{2,1,0:T(8,128)(2,1)S(1)} async-done(((bf16[16,8,2048]{2,1,0:T(8,128)(2,1)}), bf16[16,8,2048]{2,1,0:T(8,128)(2,1)S(1)}, u32[]{:S(2)}, u32[]{:S(2)}) %all-to-all-start.1) | async-done | bytes 524320 | tf_op jit(solution)/shard_map/all_to_all | solution.py:99
  121.6 1.9 gather_fusion
  123.5 36.9 %all_to_all.45 = bf16[32,1,24,128]{3,2,1,0:T(8,128)(2,1)S(1)} all-to-all(bf16[32,1,24,128]{3,2,1,0:T(8,128)(2,1)S(1)} %bitcast.418), channel_id=1, replica_groups=mesh['sp_0'=16,'sp_1'=2,'tp'=16] {'sp_0','sp_1'}, dimensions={0} | all-to-all | bytes 393216 | tf_op jit(solution)/shard_map/all_to_all | solution.py:306
  160.4 0.6 broadcast_in_dim.57
  161.0 41.0 %all_to_all.46 = bf16[16,32,1,24,128]{4,3,1,2,0:T(8,128)(2,1)S(1)} all-to-all(bf16[16,32,1,24,128]{4,3,1,2,0:T(8,128)(2,1)S(1)} %broadcast_in_dim.57), channel_id=1, replica_groups=mesh['sp_0'=16,'sp_1'=2,'tp'=16] {'tp'}, dimensions={0} | all-to-all | bytes 6291456 | tf_op jit(solution)/shard_map/all_to_all | solution.py:99
  202.0 5.3 %copy.165 = bf16[32,1,24,16,128]{4,3,2,0,1:T(8,128)(2,1)} copy(bf16[32,1,24,16,128]{4,2,0,1,3:T(8,128)(2,1)S(1)} %bitcast.407) | data formatting | bytes 6291456 | tf_op jit(solution)/shard_map/transpose | solution.py:92
  207.4 5.9 %reshape.1276 = bf16[32,24,2048]{2,1,0:T(8,128)(2,1)} reshape(bf16[32,1,24,16,128]{4,3,2,0,1:T(8,128)(2,1)} %copy.165) | data formatting | bytes 6291456 | tf_op jit(solution)/shard_map/reshape.292
  213.3 2.9 convolution_bitcast_fusion.1
  216.2 7.0 %fusion = bf16[32,1,24,2048]{3,2,0,1:T(8,128)(2,1)} fusion(bf16[32,24,2048]{2,1,0:T(8,128)(2,1)} %reshape.1276, bf16[1,128,2048]{2,1,0:T(8,128)(2,1)S(1)} %copy-done, bf16[1,2048,128]{2,1,0:T(8,128)(2,1)S(1)} %copy-done.6, f32[32,1,24,128]{3,2,0,1:T(8,128)S(1)} %convolution_bitcast_fusion.1), kind=kOutput, calls=%fused_computation.5 | convolution fusion | flops 807469056 | bytes 7733248 | tf_op jit(solution)/shard_map/secf,efd->secd/dot_general | solution.py:316
  223.2 2.7 bitcast_bitcast_fusion
  225.9 41.9 %all_to_all.47 = bf16[16,32,1,24,128]{4,3,1,2,0:T(8,128)(2,1)} all-to-all(bf16[16,32,1,24,128]{4,3,1,2,0:T(8,128)(2,1)S(1)} %bitcast_bitcast_fusion), channel_id=1, replica_groups=mesh['sp_0'=16,'sp_1'=2,'tp'=16] {'tp'}, dimensions={0} | all-to-all | bytes 6291456 | tf_op jit(solution)/shard_map/all_to_all | solution.py:87
  267.8 3.2 reduce_sum.84
  270.9 6.7 %all-to-all-start.6 = ((bf16[32,1,24,128]{3,2,1,0:T(8,128)(2,1)}), bf16[32,1,24,128]{3,2,1,0:T(8,128)(2,1)S(1)}, u32[]{:S(2)}, u32[]{:S(2)}) async-start(bf16[32,1,24,128]{3,2,1,0:T(8,128)(2,1)} %bitcast.140), calls=%async_computation.6 | async-start | bytes 393216 | tf_op jit(solution)/shard_map/all_to_all | solution.py:321
  277.9 0.3 fusion.180
  278.2 1.3 convolution_convert_fusion.1
  279.5 17.1 %all-to-all-done.6 = bf16[32,1,24,128]{3,2,1,0:T(8,128)(2,1)S(1)} async-done(((bf16[32,1,24,128]{3,2,1,0:T(8,128)(2,1)}), bf16[32,1,24,128]{3,2,1,0:T(8,128)(2,1)S(1)}, u32[]{:S(2)}, u32[]{:S(2)}) %all-to-all-start.6) | async-done | bytes 196640 | tf_op jit(solution)/shard_map/all_to_all | solution.py:321
  296.6 3.6 %all-to-all-start.2 = ((bf16[16,8,2048]{2,1,0:T(8,128)(2,1)}), bf16[16,8,2048]{2,1,0:T(8,128)(2,1)S(1)}, u32[]{:S(2)}, u32[]{:S(2)}) async-start(bf16[16,8,2048]{2,1,0:T(8,128)(2,1)} %bitcast.113), calls=%async_computation.2 | async-start | bytes 1048576 | tf_op jit(solution)/shard_map/all_to_all | solution.py:87
  300.3 1.0 gather_fusion.1
  301.3 0.9 multiply_reduce_fusion
  302.2 8.3 %all-to-all-done.2 = bf16[16,8,2048]{2,1,0:T(8,128)(2,1)S(1)} async-done(((bf16[16,8,2048]{2,1,0:T(8,128)(2,1)}), bf16[16,8,2048]{2,1,0:T(8,128)(2,1)S(1)}, u32[]{:S(2)}, u32[]{:S(2)}) %all-to-all-start.2) | async-done | bytes 524320 | tf_op jit(solution)/shard_map/all_to_all | solution.py:87
  310.5 3.5 %all-to-all-start.7 = ((bf16[16,8,128]{2,1,0:T(8,128)(2,1)}), bf16[16,8,128]{2,1,0:T(8,128)(2,1)S(1)}, u32[]{:S(2)}, u32[]{:S(2)}) async-start(bf16[16,8,128]{2,1,0:T(8,128)(2,1)} %bitcast.388), calls=%async_computation.7 | async-start | bytes 65536 | tf_op jit(solution)/shard_map/all_to_all | solution.py:328
  314.1 6.3 %all-to-all-done.7 = bf16[16,8,128]{2,1,0:T(8,128)(2,1)S(1)} async-done(((bf16[16,8,128]{2,1,0:T(8,128)(2,1)}), bf16[16,8,128]{2,1,0:T(8,128)(2,1)S(1)}, u32[]{:S(2)}, u32[]{:S(2)}) %all-to-all-start.7) | async-done | bytes 32800 | tf_op jit(solution)/shard_map/all_to_all | solution.py:328
  320.4 0.6 fusion.63
  (182 shorter events, 8.9 us)
Async XLA Ops:
  0.0 216.2 %copy-start = (bf16[1,128,2048]{2,1,0:T(8,128)(2,1)S(1)}, bf16[1,128,2048]{2,1,0:T(8,128)(2,1)}, u32[]{:S(2)}) copy-start(bf16[1,128,2048]{2,1,0:T(8,128)(2,1)} %param.38) | copy-start | bytes 1572868
  2.3 15.0 %collective-permute-start = (bf16[2,384]{0,1:T(8,128)(2,1)S(1)}, bf16[2,384]{0,1:T(8,128)(2,1)S(1)}, u32[]{:S(2)}, u32[]{:S(2)}) collective-permute-start(bf16[2,384]{0,1:T(8,128)(2,1)S(1)} %get-tuple-element.50), channel_id=1, source_target_pairs={{0,16},{16,32},{32,48},{48,64},{64,80},{80,96},{96,112},{112,128},... | collective-permute-start | bytes 4616 | tf_op jit(solution)/shard_map/ppermute | solution.py:25
  7.2 10.1 %collective-permute-start.1 = (bf16[2,384]{0,1:T(8,128)(2,1)S(1)}, bf16[2,384]{0,1:T(8,128)(2,1)S(1)}, u32[]{:S(2)}, u32[]{:S(2)}) collective-permute-start(bf16[2,384]{0,1:T(8,128)(2,1)S(1)} %get-tuple-element.51), channel_id=1, source_target_pairs={{16,0},{32,16},{48,32},{64,48},{80,64},{96,80},{112,96},{128,112},... | collective-permute-start | bytes 4616 | tf_op jit(solution)/shard_map/ppermute | solution.py:27
  18.4 72.3 %copy-start.7 = (bf16[128,128]{1,0:T(8,128)(2,1)S(1)}, bf16[128,128]{1,0:T(8,128)(2,1)}, u32[]{:S(2)}) copy-start(bf16[128,128]{1,0:T(8,128)(2,1)} %param.23) | copy-start | bytes 98308
  19.1 72.0 %copy-start.1 = (bf16[128,2048]{1,0:T(8,128)(2,1)S(1)}, bf16[128,2048]{1,0:T(8,128)(2,1)}, u32[]{:S(2)}) copy-start(bf16[128,2048]{1,0:T(8,128)(2,1)} %param.32) | copy-start | bytes 1572868
  19.1 72.0 %copy-start.11 = (f32[128]{0:T(128)S(1)}, f32[128]{0:T(128)}, u32[]{:S(2)}) copy-start(f32[128]{0:T(128)} %param.31) | copy-start | bytes 1540
  63.6 44.4 %copy-start.8 = (bf16[8,2048]{1,0:T(8,128)(2,1)S(1)}, bf16[8,2048]{1,0:T(8,128)(2,1)}, u32[]{:S(2)}) copy-start(bf16[8,2048]{1,0:T(8,128)(2,1)} %param.21) | copy-start | bytes 98308
  63.6 44.5 %copy-start.9 = (f32[2048]{0:T(1024)S(1)}, f32[2048]{0:T(1024)}, u32[]{:S(2)}) copy-start(f32[2048]{0:T(1024)} %param.33) | copy-start | bytes 24580
  92.2 15.8 %all-to-all-start = ((bf16[16,8,2048]{2,1,0:T(8,128)(2,1)}), bf16[16,8,2048]{2,1,0:T(8,128)(2,1)S(1)}, u32[]{:S(2)}, u32[]{:S(2)}) async-start(bf16[16,8,2048]{2,1,0:T(8,128)(2,1)} %bitcast.111), calls=%async_computation | async-start | bytes 1048576 | tf_op jit(solution)/shard_map/all_to_all | solution.py:87
  109.1 12.5 %all-to-all-start.1 = ((bf16[16,8,2048]{2,1,0:T(8,128)(2,1)}), bf16[16,8,2048]{2,1,0:T(8,128)(2,1)S(1)}, u32[]{:S(2)}, u32[]{:S(2)}) async-start(bf16[16,8,2048]{2,1,0:T(8,128)(2,1)} %broadcast_in_dim.53), calls=%async_computation.1 | async-start | bytes 1048576 | tf_op jit(solution)/shard_map/all_to_all | solution.py:99
  207.4 5.9 %copy-start.5 = (bf16[1,2048,128]{2,1,0:T(8,128)(2,1)S(1)}, bf16[1,2048,128]{2,1,0:T(8,128)(2,1)}, u32[]{:S(2)}) copy-start(bf16[1,2048,128]{2,1,0:T(8,128)(2,1)} %param.36) | copy-start | bytes 1572868
  213.3 3.0 copy-start.6
  267.8 10.0 %copy-start.10 = (f32[128,4]{0,1:T(4,128)S(1)}, f32[128,4]{0,1:T(4,128)}, u32[]{:S(2)}) copy-start(f32[128,4]{0,1:T(4,128)} %param.35) | copy-start | bytes 6148
  267.8 10.2 %copy-start.2 = (bf16[2048,128]{1,0:T(8,128)(2,1)S(1)}, bf16[2048,128]{1,0:T(8,128)(2,1)}, u32[]{:S(2)}) copy-start(bf16[2048,128]{1,0:T(8,128)(2,1)} %param.39) | copy-start | bytes 1572868
  267.8 10.5 %copy-start.3 = (bf16[128,2048]{1,0:T(8,128)(2,1)S(1)}, bf16[128,2048]{1,0:T(8,128)(2,1)}, u32[]{:S(2)}) copy-start(bf16[128,2048]{1,0:T(8,128)(2,1)} %param.41) | copy-start | bytes 1572868
  267.8 10.5 %copy-start.4 = (bf16[2048,128]{1,0:T(8,128)(2,1)S(1)}, bf16[2048,128]{1,0:T(8,128)(2,1)}, u32[]{:S(2)}) copy-start(bf16[2048,128]{1,0:T(8,128)(2,1)} %param.40) | copy-start | bytes 1572868
  270.9 25.7 %all-to-all-start.6 = ((bf16[32,1,24,128]{3,2,1,0:T(8,128)(2,1)}), bf16[32,1,24,128]{3,2,1,0:T(8,128)(2,1)S(1)}, u32[]{:S(2)}, u32[]{:S(2)}) async-start(bf16[32,1,24,128]{3,2,1,0:T(8,128)(2,1)} %bitcast.140), calls=%async_computation.6 | async-start | bytes 393216 | tf_op jit(solution)/shard_map/all_to_all | solution.py:321
  296.6 13.9 %all-to-all-start.2 = ((bf16[16,8,2048]{2,1,0:T(8,128)(2,1)}), bf16[16,8,2048]{2,1,0:T(8,128)(2,1)S(1)}, u32[]{:S(2)}, u32[]{:S(2)}) async-start(bf16[16,8,2048]{2,1,0:T(8,128)(2,1)} %bitcast.113), calls=%async_computation.2 | async-start | bytes 1048576 | tf_op jit(solution)/shard_map/all_to_all | solution.py:87
  310.5 9.9 %all-to-all-start.7 = ((bf16[16,8,128]{2,1,0:T(8,128)(2,1)}), bf16[16,8,128]{2,1,0:T(8,128)(2,1)S(1)}, u32[]{:S(2)}, u32[]{:S(2)}) async-start(bf16[16,8,128]{2,1,0:T(8,128)(2,1)} %bitcast.388), calls=%async_computation.7 | async-start | bytes 65536 | tf_op jit(solution)/shard_map/all_to_all | solution.py:328
where the time goes:
time: 323 us; the launch traced here: 321 us
  blocking collectives  182 us (56%)
  waiting for transfers between devices  45.2 us (14%)
  starting transfers between devices  34.2 us (11%)
  local copies, waits for them, and re-layouts  33.9 us (10%)
  matrix products  15.5 us (5%)
  other arithmetic  9.6 us (3%)
    all_gather x4, blocking collectives, collected_together(): both, at, found = (lax.all_gather(jnp.concatenate(lines), axis), 0, {})  62 us
    all_to_all x1, blocking collectives, sum_at_owner(): lax.all_to_all(pieces, axis, split_axis=0, concat_axis=0, tiled=True)  41.9 us
    all_to_all x1, blocking collectives, sent_to_all(): lax.all_to_all(jnp.broadcast_to(value[None], (devices, *value.shape)), ax...  41 us
    all_to_all x1, blocking collectives, on_device(): lax.all_to_all(outgoing, SP, split_axis=0, concat_axis=0, tiled=True)  36.9 us
    all_to_all x1, waiting for transfers between devices, on_device(): lax.all_to_all(summed.astype(jnp.bfloat16), SP, split_axis=0, concat_axis...  17.1 us
    all_to_all x2, waiting for transfers between devices, sum_at_owner(): lax.all_to_all(pieces, axis, split_axis=0, concat_axis=0, tiled=True)  15.4 us
    all_to_all x2, starting transfers between devices, sum_at_owner(): lax.all_to_all(pieces, axis, split_axis=0, concat_axis=0, tiled=True)  10.3 us
    dot_general x1, matrix products, on_device(): jnp.einsum('secf,efd->secd', hidden, routed_down_weight, preferred_elemen...  6.97 us
  transfers between devices with their start and end apart: 7, of which 5 were waited for; matrix products, arithmetic and copies ran while one was open for 4% of the time, Pallas kernels for 0%

commit v1 on v0

--- a/solution.py
+++ b/solution.py
@@ -1,17 +1,304 @@
 import jax
 import jax.numpy as jnp
+import numpy as np
 from jax import lax
-from jax.sharding import Mesh
+from jax.experimental import pallas as pl
+from jax.experimental.pallas import tpu as pltpu
 from jax.sharding import PartitionSpec as P
 
 HD = 64
 BLK = 128
-SP = ("sp_0", "sp_1")
-SP_TP = ("sp_0", "sp_1", "tp")
-
-
+SP = "sp"
+SP_TP = ("sp", "tp")
 EPSILON = 1e-06
 HIGHEST = lax.Precision.HIGHEST
+F32 = jnp.float32
+BF16 = jnp.bfloat16
+MESH = pl.DeviceIdType.MESH
+NZ = 16
+NT = 16
+CAP = 24
+GRP = CAP // 8
+SLOTS = 2 * NZ * CAP
+CHUNKS = 4
+CG = 2 * NZ * GRP // CHUNKS
+HG = CG // 2
+OFFSETS = [0] + [s * d for d in range(1, 8) for s in (1, -1)] + [8]
+PLACE = {d % NZ: k for k, d in enumerate(OFFSETS)}
+
+
+def place_back(d):
+    return PLACE[(-d) % NZ]
+
+
+def slot_facts():
+    slot = np.arange(SLOTS)
+    place = slot // CAP
+    facts = np.zeros((8, SLOTS), np.int32)
+    facts[0] = np.array(OFFSETS)[place // 2] % NZ
+    facts[1] = place % 2
+    facts[2] = slot % CAP
+    return facts
+
+
+def remote(src, dst, send, recv, sp, tp):
+    copy = pltpu.make_async_remote_copy(
+        src_ref=src, dst_ref=dst, send_sem=send, recv_sem=recv, device_id=(sp, tp), device_id_type=MESH
+    )
+    copy.start()
+
+
+def await_bytes(ref, sem):
+    pltpu.make_async_copy(ref, ref, sem).wait()
+
+
+def flat(cells):
+    return cells.astype(F32).reshape(-1, cells.shape[-1]).astype(BF16)
+
+
+def tiles(values):
+    return values.reshape(-1, 8, values.shape[-1]).astype(BF16)
+
+
+def mm(a, b):
+    return jnp.dot(a, b, preferred_element_type=F32)
+
+
+def mm_t(a, b):
+    return lax.dot_general(a, b, (((0,), (0,)), ((), ())), preferred_element_type=F32)
+
+
+def moe_kernel(
+    rows_in, resid, facts, expert_id, expert_w, wg, wu, wd, cg, cu, cd, out,
+    w_gu, w_d, c_gu, c_d, outgoing, x_all, y_all, shared_out, shared_in,
+    part_a, part_b, sum_a, sum_b, two_a, two_b, final, back, last_out, last_in,
+    sem_w, z_send, z_recv, p_send, a1_recv, b1_recv, a2_recv, b2_recv,
+    ra1_recv, rb1_recv, ra2_recv, rb2_recv, back_send, back_recv, sh_send, sh_recv, l_send, l_recv,
+):
+    sp = lax.axis_index("sp")
+    tp = lax.axis_index("tp")
+    z, core = sp // 2, sp % 2
+    y, x = tp // 4, tp % 4
+    loads = [
+        pltpu.make_async_copy(wg.at[0], w_gu.at[:, 0:128], sem_w.at[0]),
+        pltpu.make_async_copy(wu.at[0], w_gu.at[:, 128:256], sem_w.at[1]),
+        pltpu.make_async_copy(wd.at[0], w_d, sem_w.at[2]),
+        pltpu.make_async_copy(cg, c_gu.at[:, 0:128], sem_w.at[3]),
+        pltpu.make_async_copy(cu, c_gu.at[:, 128:256], sem_w.at[4]),
+        pltpu.make_async_copy(cd, c_d, sem_w.at[5]),
+    ]
+    for load in loads:
+        load.start()
+
+    def chip(d, c):
+        return lax.rem(z + d + NZ, NZ) * 2 + c
+
+    def plane(dx, dy):
+        return lax.rem(y + dy, 4) * 4 + lax.rem(x + dx, 4)
+
+    steps = [(dx, dy) for dx in range(4) for dy in range(4) if dx or dy]
+    barrier = pltpu.get_barrier_semaphore()
+    for d in OFFSETS:
+        if d:
+            for c in range(2):
+                pl.semaphore_signal(barrier, inc=1, device_id=(chip(d, c), tp), device_id_type=MESH)
+    pl.semaphore_signal(barrier, inc=1, device_id=(chip(0, 1 - core), tp), device_id_type=MESH)
+    for dx, dy in steps:
+        pl.semaphore_signal(barrier, inc=1, device_id=(sp, plane(dx, dy)), device_id_type=MESH)
+
+    expert_of = 2 * ((facts[0:1, :] + z) & (NZ - 1)) + facts[1:2, :]
+    named = jnp.zeros((128, SLOTS), jnp.bool_)
+    weight_of = jnp.zeros((128, SLOTS), F32)
+    for k in range(4):
+        hit = expert_id[:, k : k + 1] == expert_of
+        weight_of = weight_of + jnp.where(hit, expert_w[:, k : k + 1], 0.0)
+        named = named | hit
+    row = lax.broadcasted_iota(jnp.int32, (128, 128), 0)
+    col = lax.broadcasted_iota(jnp.int32, (128, 128), 1)
+    below = jnp.where(col < row, 1.0, 0.0).astype(BF16)
+    place = mm(below, jnp.where(named, 1.0, 0.0).astype(BF16))
+    picked = named & (place == facts[2:3, :].astype(F32))
+    select = jnp.where(picked, 1.0, 0.0).astype(BF16)
+    weight_of = jnp.where(picked, weight_of, 0.0)
+    own = rows_in[:, pl.ds(pl.multiple_of(tp * 128, 128), 128)]
+    outgoing[...] = tiles(mm_t(select, own))
+
+    pl.semaphore_wait(barrier, 2 * NZ - 1 + NT - 1)
+
+    def slab(ref, k):
+        return ref.at[pl.ds(k * GRP, GRP)]
+
+    mine = x_all.at[y, x]
+    for place_no, d in enumerate(OFFSETS):
+        target = 2 * place_back(d) + core
+        chunk = place_back(d) * 2 // (2 * NZ // CHUNKS)
+        for c in range(2) if d else (1 - core,):
+            remote(
+                slab(outgoing, 2 * place_no + c), slab(mine, target), z_send, z_recv.at[chunk], chip(d, c), tp
+            )
+    mine[pl.ds(core * GRP, GRP)] = outgoing[pl.ds(core * GRP, GRP)]
+
+    for load in loads[3:]:
+        load.wait()
+    h = mm(rows_in[...], c_gu[...])
+    hidden = (jax.nn.silu(h[:, 0:128]) * h[:, 128:256]).astype(BF16)
+    shared_out[...] = tiles(mm(hidden, c_d[...]))
+    for dx, dy in steps:
+        peer = plane(dx, dy)
+        remote(shared_out.at[peer], shared_in.at[tp], sh_send, sh_recv, sp, peer)
+    for load in loads[:3]:
+        load.wait()
+
+    def gather_one(k):
+        got = 2 * NZ // CHUNKS * GRP - (GRP if k == 0 else 0)
+        await_bytes(y_all.at[0, 0, 0:got], z_recv.at[k])
+        a, b = pl.ds(k * CG, HG), pl.ds(k * CG + HG, HG)
+        for s in range(1, 4):
+            remote(x_all.at[y, x, a], x_all.at[y, x, a], p_send.at[k, 0], a1_recv.at[k], sp, plane(s, 0))
+            remote(x_all.at[y, x, b], x_all.at[y, x, b], p_send.at[k, 1], b1_recv.at[k], sp, plane(0, s))
+
+    def gather_two(k):
+        a, b = pl.ds(k * CG, HG), pl.ds(k * CG + HG, HG)
+        await_bytes(y_all.at[0, 0, 0 : 3 * HG], a1_recv.at[k])
+        for s in range(1, 4):
+            remote(x_all.at[y, :, a], x_all.at[y, :, a], p_send.at[k, 2], a2_recv.at[k], sp, plane(0, s))
+        await_bytes(y_all.at[0, 0, 0 : 3 * HG], b1_recv.at[k])
+        for s in range(1, 4):
+            remote(x_all.at[:, x, b], x_all.at[:, x, b], p_send.at[k, 3], b2_recv.at[k], sp, plane(s, 0))
+
+    def experts(k):
+        await_bytes(y_all.at[0, 0:3, 0 : 4 * HG], a2_recv.at[k])
+        await_bytes(y_all.at[0, 0:3, 0 : 4 * HG], b2_recv.at[k])
+        at = pl.ds(k * CG, CG)
+        total = jnp.zeros((CG * 8, 256), F32)
+        for j in range(0, NT, 2):
+            left = jnp.concatenate(
+                [flat(x_all[j // 4, j % 4, at]), flat(x_all[j // 4, j % 4 + 1, at])], axis=1
+            )
+            total = total + mm(left, w_gu[j * 128 : (j + 2) * 128, :])
+        mid = (jax.nn.silu(total[:, 0:128]) * total[:, 128:256]).astype(BF16)
+        for j in range(0, NT, 2):
+            part = mm(mid, w_d[:, j * 128 : (j + 2) * 128])
+            y_all[j // 4, j % 4, at] = tiles(part[:, 0:128])
+            y_all[j // 4, j % 4 + 1, at] = tiles(part[:, 128:256])
+        a, b = pl.ds(k * CG, HG), pl.ds(k * CG + HG, HG)
+        for s in range(1, 4):
+            peer_y, peer_x = lax.rem(y + s, 4), lax.rem(x + s, 4)
+            remote(y_all.at[peer_y, :, a], part_a.at[k, s - 1], p_send.at[k, 4], ra1_recv.at[k], sp, plane(0, s))
+            remote(y_all.at[:, peer_x, b], part_b.at[k, s - 1], p_send.at[k, 5], rb1_recv.at[k], sp, plane(s, 0))
+
+    def reduce_one(k):
+        a, b = pl.ds(k * CG, HG), pl.ds(k * CG + HG, HG)
+        await_bytes(part_a.at[k], ra1_recv.at[k])
+        for i in range(4):
+            total = y_all[y, i, a].astype(F32)
+            for s in range(3):
+                total = total + part_a[k, s, i].astype(F32)
+            sum_a[k, i] = total.astype(BF16)
+        for s in range(1, 4):
+            remote(sum_a.at[k, lax.rem(x + s, 4)], two_a.at[k, s - 1], p_send.at[k, 6], ra2_recv.at[k], sp, plane(s, 0))
+        await_bytes(part_b.at[k], rb1_recv.at[k])
+        for i in range(4):
+            total = y_all[i, x, b].astype(F32)
+            for s in range(3):
+                total = total + part_b[k, s, i].astype(F32)
+            sum_b[k, i] = total.astype(BF16)
+        for s in range(1, 4):
+            remote(sum_b.at[k, lax.rem(y + s, 4)], two_b.at[k, s - 1], p_send.at[k, 7], rb2_recv.at[k], sp, plane(0, s))
+
+    def reduce_two(k):
+        await_bytes(two_a.at[k], ra2_recv.at[k])
+        await_bytes(two_b.at[k], rb2_recv.at[k])
+        total_a = sum_a[k, x].astype(F32)
+        total_b = sum_b[k, y].astype(F32)
+        for s in range(3):
+            total_a = total_a + two_a[k, s].astype(F32)
+            total_b = total_b + two_b[k, s].astype(F32)
+        final[pl.ds(k * CG, HG)] = total_a.astype(BF16)
+        final[pl.ds(k * CG + HG, HG)] = total_b.astype(BF16)
+        per = NZ // CHUNKS
+        for place_no in range(k * per, k * per + per):
+            d = OFFSETS[place_no]
+            target = 2 * place_back(d) + core
+            for c in range(2) if d else (1 - core,):
+                remote(slab(final, 2 * place_no + c), slab(back, target), back_send, back_recv, chip(d, c), tp)
+        if k == 0:
+            back[pl.ds(core * GRP, GRP)] = final[pl.ds(core * GRP, GRP)]
+
+    stages = (gather_one, gather_two, experts, reduce_one, reduce_two)
+    for t in range(CHUNKS + len(stages) - 1):
+        for number, stage in enumerate(stages):
+            if 0 <= t - number < CHUNKS:
+                stage(t - number)
+
+    high = weight_of.astype(BF16)
+    low = (weight_of - high.astype(F32)).astype(BF16)
+    await_bytes(back.at[0 : (2 * NZ - 1) * GRP], back_recv)
+    returned = flat(back[...])
+    last_out[...] = tiles(mm(high, returned) + mm(low, returned))
+    for dx, dy in steps:
+        peer = plane(dx, dy)
+        remote(last_out.at[peer], last_in.at[tp], l_send, l_recv, sp, peer)
+    last_in[tp] = last_out[tp]
+    shared_in[tp] = shared_out[tp]
+    await_bytes(shared_in.at[0 : NT - 1], sh_recv)
+    total = resid[...].astype(F32)
+    total = total + jnp.sum(shared_in[...].astype(F32), axis=0)
+    await_bytes(last_in.at[0 : NT - 1], l_recv)
+    for j in range(NT):
+        at = slice(j * 128, (j + 1) * 128)
+        out[:, at] = (total[:, at] + last_in[j].astype(F32)).astype(BF16)
+    await_bytes(outgoing.at[0 : (2 * NZ - 1) * GRP], z_send)
+    await_bytes(outgoing.at[0 : (2 * NZ - 1) * GRP], back_send)
+    await_bytes(shared_in.at[0 : NT - 1], sh_send)
+    await_bytes(last_in.at[0 : NT - 1], l_send)
+    for k in range(CHUNKS):
+        for kind in (0, 1, 6, 7):
+            await_bytes(two_a.at[k], p_send.at[k, kind])
+        for kind in (2, 3, 4, 5):
+            await_bytes(part_a.at[k], p_send.at[k, kind])
+
+
+def moe(rows, resid, expert_id, expert_w, weights):
+    vmem = pl.BlockSpec(memory_space=pltpu.VMEM)
+    anywhere = pl.BlockSpec(memory_space=pl.ANY)
+    dma = pltpu.SemaphoreType.DMA
+    all_groups = 2 * NZ * GRP
+    return pl.pallas_call(
+        moe_kernel,
+        name="moe",
+        out_shape=jax.ShapeDtypeStruct((8, 2048), BF16),
+        in_specs=[vmem] * 5 + [anywhere] * 6,
+        out_specs=vmem,
+        scratch_shapes=[
+            pltpu.VMEM((2048, 256), BF16),
+            pltpu.VMEM((128, 2048), BF16),
+            pltpu.VMEM((2048, 256), BF16),
+            pltpu.VMEM((128, 2048), BF16),
+            pltpu.VMEM((all_groups, 8, 128), BF16),
+            pltpu.VMEM((4, 4, all_groups, 8, 128), BF16),
+            pltpu.VMEM((4, 4, all_groups, 8, 128), BF16),
+            pltpu.VMEM((NT, 8, 2048), BF16),
+            pltpu.VMEM((NT, 8, 2048), BF16),
+            pltpu.VMEM((CHUNKS, 3, 4, HG, 8, 128), BF16),
+            pltpu.VMEM((CHUNKS, 3, 4, HG, 8, 128), BF16),
+            pltpu.VMEM((CHUNKS, 4, HG, 8, 128), BF16),
+            pltpu.VMEM((CHUNKS, 4, HG, 8, 128), BF16),
+            pltpu.VMEM((CHUNKS, 3, HG, 8, 128), BF16),
+            pltpu.VMEM((CHUNKS, 3, HG, 8, 128), BF16),
+            pltpu.VMEM((all_groups, 8, 128), BF16),
+            pltpu.VMEM((all_groups, 8, 128), BF16),
+            pltpu.VMEM((NT, 8, 128), BF16),
+            pltpu.VMEM((NT, 8, 128), BF16),
+            dma((6,)), dma, dma((CHUNKS,)), dma((CHUNKS, 8)),
+            dma((CHUNKS,)), dma((CHUNKS,)), dma((CHUNKS,)), dma((CHUNKS,)),
+            dma((CHUNKS,)), dma((CHUNKS,)), dma((CHUNKS,)), dma((CHUNKS,)),
+            dma, dma, dma, dma, dma, dma,
+        ],
+        compiler_params=pltpu.CompilerParams(
+            collective_id=1, has_side_effects=True, vmem_limit_bytes=48 << 20
+        ),
+    )(rows, resid, jnp.asarray(slot_facts()), expert_id, expert_w, *weights)
 
 
 def padded_2(cells, sides, width):
@@ -57,7 +344,7 @@
 def entering(value, axes, combine, identity, reverse):
     before = start = neutral_like(value, identity)
     running = value
-    for axis in reversed(axes):
+    for axis in (axes,):
         devices, index = (lax.axis_size(axis), lax.axis_index(axis))
         pieces = collected_together(
             jax.tree.map(
@@ -152,21 +439,6 @@
         last_state,
         through,
     )
-
-
-def slot_table(expert_ids, experts, capacity):
-    row_count, top_count = expert_ids.shape
-    flat_ids = expert_ids.reshape(-1)
-    one_hot = (flat_ids[:, None] == jnp.arange(experts, dtype=jnp.int32)[None, :]).astype(jnp.int32)
-    earlier = jnp.cumsum(one_hot, axis=0) - one_hot
-    position = jnp.sum(earlier * one_hot, axis=1)
-    owners = jnp.arange(row_count * top_count, dtype=jnp.int32) // top_count
-    table = (
-        jnp.full((experts * capacity,), row_count, jnp.int32)
-        .at[flat_ids * capacity + position]
-        .set(owners)
-    )
-    return (position.reshape(row_count, top_count), table)
 
 
 def combine_states(earlier, later):
@@ -289,62 +561,23 @@
         * feedforward_norm_gain
     ).astype(jnp.bfloat16)
     all_rows = gather_directly(normed, "tp", 0)
-    sp_count = lax.axis_size(SP)
-    local_experts = routed_gate_weight.shape[0]
-    experts = local_experts * sp_count
-    top_count = routed_expert_index.shape[1]
-    capacity = 3 * seq_rows * top_count // (2 * experts)
-    model_width = all_rows.shape[1]
-    position, table = slot_table(routed_expert_index, experts, capacity)
-    padded_rows = jnp.concatenate([all_rows, jnp.zeros((1, model_width), jnp.bfloat16)], axis=0)
-    column_width = model_width // lax.axis_size("tp")
-    own_columns = lax.dynamic_slice_in_dim(
-        padded_rows, lax.axis_index("tp") * column_width, column_width, 1
-    )
-    outgoing = own_columns[table].reshape(sp_count, local_experts, capacity, column_width)
-    piece = gather_directly(
-        lax.all_to_all(outgoing, SP, split_axis=0, concat_axis=0, tiled=True), "tp", 3
-    )
-    gate_part = jnp.einsum(
-        "secd,edf->secf", piece, routed_gate_weight, preferred_element_type=jnp.float32
-    )
-    up_part = jnp.einsum(
-        "secd,edf->secf", piece, routed_up_weight, preferred_element_type=jnp.float32
-    )
-    hidden = (jax.nn.silu(gate_part) * up_part).astype(jnp.bfloat16)
-    partial_value = lax.optimization_barrier(
-        jnp.einsum(
-            "secf,efd->secd", hidden, routed_down_weight, preferred_element_type=jnp.float32
-        ).astype(jnp.bfloat16)
-    ).astype(jnp.float32)
-    summed = sum_at_owner(partial_value.astype(jnp.bfloat16), "tp", 3)
-    returned = lax.all_to_all(
-        summed.astype(jnp.bfloat16), SP, split_axis=0, concat_axis=0, tiled=True
-    ).astype(summed.dtype)
-    slot_index = routed_expert_index * capacity + position
-    flat_back = returned.reshape(experts * capacity, returned.shape[3])
-    chosen = flat_back[slot_index]
-    routed = jnp.sum(routed_expert_weight[..., None] * chosen, axis=1)
-    routed_part = lax.all_to_all(
-        routed.astype(jnp.bfloat16), "tp", split_axis=0, concat_axis=1, tiled=True
-    ).astype(routed.dtype)
-    picked_rows = all_rows
-    gate_part = jnp.dot(picked_rows, common_gate_weight, preferred_element_type=jnp.float32)
-    up_part = jnp.dot(picked_rows, common_up_weight, preferred_element_type=jnp.float32)
-    hidden = (jax.nn.silu(gate_part) * up_part).astype(jnp.bfloat16)
-    shared_part = sum_at_owner(
-        rounded(jnp.dot(hidden, common_down_weight, preferred_element_type=jnp.float32)).astype(
-            jnp.bfloat16
+    return moe(
+        all_rows,
+        residual,
+        routed_expert_index,
+        routed_expert_weight,
+        (
+            routed_gate_weight,
+            routed_up_weight,
+            routed_down_weight,
+            common_gate_weight,
+            common_up_weight,
+            common_down_weight,
         ),
-        "tp",
-        0,
-    )
-    feed = shared_part + routed_part
-    return (widened + feed).astype(jnp.bfloat16)
+    )
 
 
 def solution(mesh):
-    finer = Mesh(mesh.devices.reshape(16, 2, mesh.shape["tp"]), ("sp_0", "sp_1", "tp"))
     placed = (
         P(SP_TP, None),
         P(SP, "tp"),
@@ -369,5 +602,5 @@
         P("tp", None),
     )
     return jax.shard_map(
-        on_device, mesh=finer, in_specs=placed, out_specs=P(SP_TP, None), check_vma=False
-    )
+        on_device, mesh=mesh, in_specs=placed, out_specs=P(SP_TP, None), check_vma=False
+    )

time: 323 us -> 302 us (0.935)
  blocking collectives: 182 us -> 17.1 us
  waiting for transfers between devices: 45.2 us -> 148 us
  Pallas kernels: 0 us -> 78.8 us
  starting transfers between devices: 34.2 us -> 13.8 us
  local copies, waits for them, and re-layouts: 33.9 us -> 20.3 us
  between operations: 0.85 us -> 14.1 us
  matrix products: 15.5 us -> 3.16 us
    all_gather x0 -> x2, waiting for transfers between devices: none -> 138 us  [collected_together(): both, at, found = (lax.all_gather(jnp.concatenate(lines), axis), 0, {})]
    pallas_call x0 -> x1, Pallas kernels: none -> 78.8 us  [moe(): pl.pallas_call(moe_kernel, name='moe', out_shape=jax.ShapeDtypeStruct((8,...]
    all_to_all x2 -> x0, blocking collectives: 77.9 us -> none  [the longest x1 41 us: sent_to_all(): lax.all_to_all(jnp.broadcast_to(value[None], (devices, *value.shape)), ax...]
    all_gather x4 -> x0, blocking collectives: 62 us -> none  [collected_together(): both, at, found = (lax.all_gather(jnp.concatenate(lines), axis), 0, {})]
    all_to_all x4 -> x0, waiting for transfers between devices: 38.8 us -> none  [the longest x1 17.1 us: on_device(): lax.all_to_all(summed.astype(jnp.bfloat16), SP, split_axis=0, concat_axis...]
    all_to_all x1, blocking collectives: 41.9 us -> 17.1 us  [sum_at_owner(): lax.all_to_all(pieces, axis, split_axis=0, concat_axis=0, tiled=True)]
    all_to_all x4 -> x0, starting transfers between devices: 20.6 us -> none  [the longest x2 10.3 us: sum_at_owner(): lax.all_to_all(pieces, axis, split_axis=0, concat_axis=0, tiled=True)]
    dot_general x4 -> x0, matrix products: 11.5 us -> none  [the longest x1 6.97 us: on_device(): jnp.einsum('secf,efd->secd', hidden, routed_down_weight, preferred_elemen...]
  transfers between devices with their start and end apart: 7 -> 5, of which waited for: 5 -> 3; matrix products, arithmetic and copies ran while one was open for 4% -> 3% of each run, Pallas kernels for 0% -> 0%
where the time goes in v1:
time: 302 us
  waiting for transfers between devices  148 us (49%)
  Pallas kernels  78.8 us (26%)
  local copies, waits for them, and re-layouts  20.3 us (7%)
  blocking collectives  17.1 us (6%)
  between operations  14.1 us (5%)
  starting transfers between devices  13.8 us (5%)
  other arithmetic  6.45 us (2%)
  matrix products  3.16 us (1%)
    all_gather x2, waiting for transfers between devices, collected_together(): both, at, found = (lax.all_gather(jnp.concatenate(lines), axis), 0, {})  138 us
    pallas_call x1, Pallas kernels, moe(): pl.pallas_call(moe_kernel, name='moe', out_shape=jax.ShapeDtypeStruct((8,...  78.8 us
    all_to_all x1, blocking collectives, sum_at_owner(): lax.all_to_all(pieces, axis, split_axis=0, concat_axis=0, tiled=True)  17.1 us
    mul x128, local copies, waits for them, and re-layouts, combine_states(): jnp.exp(later[0])[..., None, None] * earlier[1] + later[1]  9.8 us
    all_to_all x1, waiting for transfers between devices, sent_to_all(): lax.all_to_all(jnp.broadcast_to(value[None], (devices, *value.shape)), ax...  9.65 us
  transfers between devices with their start and end apart: 5, of which 3 were waited for; matrix products, arithmetic and copies ran while one was open for 3% of the time, Pallas kernels for 0%

profile of v1, /device:TPU:1, one launch (start us, length us, event | category | flops | bytes accessed | tf_op | source)
XLA Modules:
  0.0 301.6 jit_solution(12211205667190484415)
XLA Ops:
  6.5 1.2 constant_dynamic-slice_fusion
  7.7 0.1 copy.143
  7.8 0.9 copy.129
  8.7 0.1 fusion.23
  8.8 4.9 %collective-permute-start = (bf16[2,384]{0,1:T(8,128)(2,1)S(1)}, bf16[2,384]{0,1:T(8,128)(2,1)S(1)}, u32[]{:S(2)}, u32[]{:S(2)}) collective-permute-start(bf16[2,384]{0,1:T(8,128)(2,1)S(1)} %get-tuple-element.50), channel_id=1, source_target_pairs={{0,16},{16,32},{32,48},{48,64},{64,80},{80,96},{96,112},{112,128},... | collective-permute-start | bytes 4616 | tf_op jit(solution)/shard_map/ppermute | solution.py:312
  13.7 5.1 %collective-permute-start.1 = (bf16[2,384]{0,1:T(8,128)(2,1)S(1)}, bf16[2,384]{0,1:T(8,128)(2,1)S(1)}, u32[]{:S(2)}, u32[]{:S(2)}) collective-permute-start(bf16[2,384]{0,1:T(8,128)(2,1)S(1)} %get-tuple-element.51), channel_id=1, source_target_pairs={{16,0},{32,16},{48,32},{64,48},{80,64},{96,80},{112,96},{128,112},... | collective-permute-start | bytes 4616 | tf_op jit(solution)/shard_map/ppermute | solution.py:314
  18.9 0.7 exp.423
  19.6 0.8 multiply_subtract_fusion
  20.4 0.1 copy.133
  20.5 0.1 fusion.204
  20.7 0.8 dynamic-slice_reduce_fusion
  21.7 0.1 maximum_maximum_fusion
  21.8 0.4 divide_multiply_fusion
  22.3 0.3 fusion.11
  22.5 0.6 maximum_bitcast_fusion
  23.2 0.1 rev.22
  23.3 0.1 copy.137
  23.4 0.1 fusion.205
  23.9 0.1 copy.144
  24.0 0.2 fusion.12
  24.2 0.6 maximum_bitcast_fusion.1
  25.0 0.1 copy.140
  25.1 0.3 convolution_bitcast_fusion.7
  25.4 0.1 copy.132
  25.5 0.1 copy.145
  25.6 0.3 convolution_bitcast_fusion.3
  25.9 0.1 copy.136
  26.0 0.3 fusion.8
  26.3 0.4 fusion.1
  26.7 0.2 fusion.4
  26.9 0.4 fusion.3
  27.4 69.0 %all-gather.7.cloned.1.call-done = bf16[32,129,128]{2,1,0:T(8,128)(2,1)} async-done(((bf16[1,129,128]{2,1,0:T(8,128)(2,1)}), bf16[32,129,128]{2,1,0:T(8,128)(2,1)}) %all-gather.7.cloned.1.call-update) | async-done | bytes 1056784 | tf_op jit(solution)/shard_map/all_gather | solution.py:335
  96.4 0.9 slice.890
  97.4 69.1 %all-gather.9.cloned.1.call-done = bf16[32,129,128]{2,1,0:T(8,128)(2,1)} async-done(((bf16[1,129,128]{2,1,0:T(8,128)(2,1)}), bf16[32,129,128]{2,1,0:T(8,128)(2,1)}) %all-gather.9.cloned.1.call-update) | async-done | bytes 1056784 | tf_op jit(solution)/shard_map/all_gather | solution.py:335
  166.5 0.8 slice.958
  167.5 0.1 mul.1468
  167.8 0.1 mul.1528
  168.1 0.1 mul.1536
  168.4 0.1 mul.1544
  168.7 0.1 mul.1552
  169.0 0.1 mul.1560
  169.3 0.1 mul.1568
  169.7 0.1 mul.1576
  170.0 0.1 mul.1584
  170.3 0.1 mul.1593
  170.4 0.1 mul.1472
  170.7 0.1 mul.1480
  177.3 1.9 select_select_fusion
  179.2 0.3 fusion.10
  179.5 0.9 select_select_fusion.1
  180.4 0.2 fusion.7
  180.7 0.1 fusion.38
  180.8 0.3 convolution_convert_fusion
  181.2 17.1 %all_to_all.10 = bf16[16,8,2048]{2,1,0:T(8,128)(2,1)S(1)} all-to-all(bf16[16,8,2048]{2,1,0:T(8,128)(2,1)S(1)} %bitcast.325), channel_id=1, replica_groups=mesh['sp'=32,'tp'=16] {'tp'}, dimensions={0} | all-to-all | bytes 1048576 | tf_op jit(solution)/shard_map/all_to_all | solution.py:374
  198.5 0.1 fusion.29
  198.7 0.8 broadcast_in_dim.43
  199.5 3.8 %all-to-all-start.1 = ((bf16[16,8,2048]{2,1,0:T(8,128)(2,1)}), bf16[16,8,2048]{2,1,0:T(8,128)(2,1)S(1)}, u32[]{:S(2)}, u32[]{:S(2)}) async-start(bf16[16,8,2048]{2,1,0:T(8,128)(2,1)} %broadcast_in_dim.43), calls=%async_computation.1 | async-start | bytes 1048576 | tf_op jit(solution)/shard_map/all_to_all | solution.py:386
  203.3 0.1 copy.141.expert_id
  203.4 0.1 copy.142.expert_w
  203.6 9.7 %all-to-all-done.1 = bf16[16,8,2048]{2,1,0:T(8,128)(2,1)S(1)} async-done(((bf16[16,8,2048]{2,1,0:T(8,128)(2,1)}), bf16[16,8,2048]{2,1,0:T(8,128)(2,1)S(1)}, u32[]{:S(2)}, u32[]{:S(2)}) %all-to-all-start.1) | async-done | bytes 524320 | tf_op jit(solution)/shard_map/all_to_all | solution.py:386
  213.2 1.0 copy-done.5
  214.3 1.0 copy-done.6
  215.3 78.8 %moe.1 = bf16[8,2048]{1,0:T(8,128)(2,1)S(1)} custom-call(bf16[128,2048]{1,0:T(8,128)(2,1)S(1)} %bitcast.319, bf16[8,2048]{1,0:T(8,128)(2,1)S(1)} %get-tuple-element.34.resid, s32[8,768]{1,0:T(8,128)S(1)} %copy-done.7, s32[128,4]{1,0:T(8,128)S(1)} %copy.141.expert_id, f32[128,4]{1,0:T(8,128)S(1)} %copy.142.expert_w, bf16[1,2048,128]{2,1,0:T(8,128)(2,1)S(1)} %copy-done.1, ...), custom_call_target="tpu_custom_call" | custom-call | tf_op jit(solution)/shard_map/moe/pallas_call | solution.py:267
  294.1 0.6 copy.156
  (189 shorter events, 9.9 us)
Async XLA Ops:
  6.5 174.3 %copy-start = (bf16[128,2048]{1,0:T(8,128)(2,1)S(1)}, bf16[128,2048]{1,0:T(8,128)(2,1)}, u32[]{:S(2)}) copy-start(bf16[128,2048]{1,0:T(8,128)(2,1)} %param.33) | copy-start | bytes 1572868
  6.5 14.9 %copy-start.12 = (f32[5,128]{1,0:T(8,128)S(1)}, f32[5,128]{1,0:T(8,128)}, u32[]{:S(2)}) copy-start(f32[5,128]{1,0:T(8,128)} %param.28) | copy-start | bytes 7684
  6.5 89.9 %all-gather.7.cloned.1.call-start = ((), (), s32[]{:S(2)}) async-start(), calls=%async_computation.2 | async-start | bytes 1148928 | tf_op jit(solution)/shard_map/all_gather | solution.py:335
  8.8 12.8 %collective-permute-start = (bf16[2,384]{0,1:T(8,128)(2,1)S(1)}, bf16[2,384]{0,1:T(8,128)(2,1)S(1)}, u32[]{:S(2)}, u32[]{:S(2)}) collective-permute-start(bf16[2,384]{0,1:T(8,128)(2,1)S(1)} %get-tuple-element.50), channel_id=1, source_target_pairs={{0,16},{16,32},{32,48},{48,64},{64,80},{80,96},{96,112},{112,128},... | collective-permute-start | bytes 4616 | tf_op jit(solution)/shard_map/ppermute | solution.py:312
  13.7 7.9 %collective-permute-start.1 = (bf16[2,384]{0,1:T(8,128)(2,1)S(1)}, bf16[2,384]{0,1:T(8,128)(2,1)S(1)}, u32[]{:S(2)}, u32[]{:S(2)}) collective-permute-start(bf16[2,384]{0,1:T(8,128)(2,1)S(1)} %get-tuple-element.51), channel_id=1, source_target_pairs={{16,0},{32,16},{48,32},{64,48},{80,64},{96,80},{112,96},{128,112},... | collective-permute-start | bytes 4616 | tf_op jit(solution)/shard_map/ppermute | solution.py:314
  22.2 2.8 copy-start.9
  23.2 143.3 %all-gather.9.cloned.1.call-start = ((), (), s32[]{:S(2)}) async-start(), calls=%async_computation.3 | async-start | bytes 1148928 | tf_op jit(solution)/shard_map/all_gather | solution.py:335
  96.4 83.1 %copy-start.8 = (bf16[32,129,128]{2,1,0:T(8,128)(2,1)S(1)}, bf16[32,129,128]{2,1,0:T(8,128)(2,1)}, u32[]{:S(2)}) copy-start(bf16[32,129,128]{2,1,0:T(8,128)(2,1)} %all-gather.7.cloned.1.call-done) | copy-start | bytes 3170308
  179.2 1.6 copy-start.15
  180.8 17.6 %copy-start.10 = (bf16[8,2048]{1,0:T(8,128)(2,1)S(1)}, bf16[8,2048]{1,0:T(8,128)(2,1)}, u32[]{:S(2)}) copy-start(bf16[8,2048]{1,0:T(8,128)(2,1)} %param.22) | copy-start | bytes 98308
  181.2 17.4 %copy-start.11 = (f32[2048]{0:T(1024)S(1)}, f32[2048]{0:T(1024)}, u32[]{:S(2)}) copy-start(f32[2048]{0:T(1024)} %param.34) | copy-start | bytes 24580
  198.3 5.0 %copy-start.13 = (s32[128,4]{0,1:T(4,128)S(1)}, s32[128,4]{0,1:T(4,128)}, u32[]{:S(2)}) copy-start(s32[128,4]{0,1:T(4,128)} %param.35) | copy-start | bytes 6148
  198.3 5.1 %copy-start.14 = (f32[128,4]{0,1:T(4,128)S(1)}, f32[128,4]{0,1:T(4,128)}, u32[]{:S(2)}) copy-start(f32[128,4]{0,1:T(4,128)} %param.36) | copy-start | bytes 6148
  198.3 14.9 %copy-start.4 = (bf16[2048,128]{1,0:T(8,128)(2,1)S(1)}, bf16[2048,128]{1,0:T(8,128)(2,1)}, u32[]{:S(2)}) copy-start(bf16[2048,128]{1,0:T(8,128)(2,1)} %cg.1) | copy-start | bytes 1572868
  198.4 14.8 %copy-start.1 = (bf16[1,2048,128]{2,1,0:T(8,128)(2,1)S(1)}, bf16[1,2048,128]{2,1,0:T(8,128)(2,1)}, u32[]{:S(2)}) copy-start(bf16[1,2048,128]{2,1,0:T(8,128)(2,1)} %wg.1) | copy-start | bytes 1572868
  198.4 14.8 %copy-start.2 = (bf16[1,2048,128]{2,1,0:T(8,128)(2,1)S(1)}, bf16[1,2048,128]{2,1,0:T(8,128)(2,1)}, u32[]{:S(2)}) copy-start(bf16[1,2048,128]{2,1,0:T(8,128)(2,1)} %wu.1) | copy-start | bytes 1572868
  198.4 14.8 %copy-start.3 = (bf16[1,128,2048]{2,1,0:T(8,128)(2,1)S(1)}, bf16[1,128,2048]{2,1,0:T(8,128)(2,1)}, u32[]{:S(2)}) copy-start(bf16[1,128,2048]{2,1,0:T(8,128)(2,1)} %wd.1) | copy-start | bytes 1572868
  198.5 14.8 %copy-start.7 = (s32[8,768]{1,0:T(8,128)S(1)}, s32[8,768]{1,0:T(8,128)}, u32[]{:S(2)}) copy-start(s32[8,768]{1,0:T(8,128)} %constant.133.clone.facts) | copy-start | bytes 73732
  199.5 13.7 %all-to-all-start.1 = ((bf16[16,8,2048]{2,1,0:T(8,128)(2,1)}), bf16[16,8,2048]{2,1,0:T(8,128)(2,1)S(1)}, u32[]{:S(2)}, u32[]{:S(2)}) async-start(bf16[16,8,2048]{2,1,0:T(8,128)(2,1)} %broadcast_in_dim.43), calls=%async_computation.1 | async-start | bytes 1048576 | tf_op jit(solution)/shard_map/all_to_all | solution.py:386
  213.2 1.0 copy-start.5
  214.3 1.0 copy-start.6
Sparse Core Ops, SparseCore 0:
  23.3 73.0 all-gather.6
  98.5 67.9 all-gather.8
